TPU v7x, 32 devices: a whole 2x2x4 slice. The times are simulated.
32 devices in a mesh: grp: 2 (over y), fs: 4 (over z), tp: 4 (over x, core).
Axes of the slice: x: 2, y: 2, z: 4, core: 2. Of those that a mesh axis runs over, the one named last changes fastest.
Arguments:
- tokens: bfloat16 [2048, 2048], P(('grp', 'fs')), parts along dimension 0, may hold values from -6 to 6
- route_ids: int32 [2048, 2], P(('grp', 'fs')), parts along dimension 0, may hold values from 0 to 7, as said below
- route_weights: float32 [2048, 2], P(('grp', 'fs')), parts along dimension 0, may hold values from 0.2 to 1
- ffn_gain: float32 [2048], P('fs'), may hold values from 0.1 to 1.9
- gate_master: float32 [8, 2048, 1024], P(None, 'fs', 'tp'), may hold values from -0.125 to 0.125
- up_master: float32 [8, 2048, 1024], P(None, 'fs', 'tp'), may hold values from -0.125 to 0.125
- down_master: float32 [8, 1024, 2048], P(None, 'fs', 'tp'), may hold values from -0.1875 to 0.1875
Outputs:
- gate_serve: bfloat16 [16, 2048, 1024], P(('grp', 'fs'), None, 'tp'), parts along dimension 0
- up_serve: bfloat16 [16, 2048, 1024], P(('grp', 'fs'), None, 'tp'), parts along dimension 0
- down_serve: bfloat16 [16, 1024, 2048], P(('grp', 'fs'), None, 'tp'), parts along dimension 0
- mixed: bfloat16 [2048, 2048], P(('grp', 'fs'), 'tp'), parts along dimension 0
There are 2 independent parts, one for each index of `grp`. A program takes and returns all parts, laid end to end along the dimension named above; an argument that names none is the same for every part. Nothing has to cross between parts.
Inputs may be any that keep to these rules, and one draw needn't show every extreme that they name: `route_ids`: each row names two different experts of one group of 8 consecutive experts. Among the tokens of one index of fs, each group is named by exactly 256 tokens and no expert by more than 128; in every group one expert, the same for every index of fs, is named by exactly 128, and so is one other expert of the group, which may change from one index of fs to the next.
All inputs are finite; a program needn't handle non-finite values.
Results may differ from a plain program's by a relative error of at most 0.0087.
Values may be sent and summed in bfloat16 or wider, within the bound.
A program may use at most 64 MiB of HBM per device.

v0:
```python
import jax
import jax.numpy as jnp
from jax import lax
from jax.sharding import PartitionSpec as P

GROUP_SIZE = 8


def slot_targets(route_ids, experts, capacity):
    flat_ids = route_ids.reshape(-1)
    member = (flat_ids[:, None] == jnp.arange(experts, dtype=jnp.int32)[None, :]).astype(jnp.int32)
    before = jnp.cumsum(member, axis=0) - member
    slot_index = jnp.sum(before * member, axis=1)
    return flat_ids * capacity + slot_index


def fill_slots(source, targets, experts, capacity):
    doubled = jnp.repeat(source, 2, axis=0)
    buffer = jnp.zeros((experts * capacity, source.shape[1]), source.dtype).at[targets].set(doubled)
    return buffer.reshape(experts, capacity, source.shape[1])


def on_device(tokens, route_ids, route_weights, ffn_gain, gate_master, up_master, down_master):
    row_gain = ffn_gain[None, :, None]
    gate_local = (gate_master * row_gain).astype(jnp.bfloat16)
    up_local = (up_master * row_gain).astype(jnp.bfloat16)
    down_local = down_master.astype(jnp.bfloat16)
    gate_serve, up_serve, down_serve = (
        lax.all_to_all(gate_local, "fs", split_axis=0, concat_axis=1, tiled=True),
        lax.all_to_all(up_local, "fs", split_axis=0, concat_axis=1, tiled=True),
        lax.all_to_all(down_local, "fs", split_axis=0, concat_axis=1, tiled=True),
    )
    experts = gate_local.shape[0]
    capacity = tokens.shape[0] // (2 * (experts // GROUP_SIZE))
    token_rows = tokens.astype(jnp.float32)
    normed = (
        token_rows * lax.rsqrt(jnp.mean(token_rows * token_rows, axis=1, keepdims=True) + 1e-06)
    ).astype(jnp.bfloat16)
    targets = slot_targets(route_ids, experts, capacity)
    col_width = normed.shape[1] // lax.axis_size("tp")
    own_cols = lax.dynamic_slice_in_dim(normed, lax.axis_index("tp") * col_width, col_width, 1)
    part_rows = lax.all_to_all(
        fill_slots(own_cols, targets, experts, capacity),
        "fs",
        split_axis=0,
        concat_axis=1,
        tiled=True,
    )
    portion = lax.all_gather(part_rows, "tp", axis=2, tiled=True)
    gate_part = jnp.einsum("erd,edf->erf", portion, gate_serve, preferred_element_type=jnp.float32)
    up_part = jnp.einsum("erd,edf->erf", portion, up_serve, preferred_element_type=jnp.float32)
    hidden = (jax.nn.silu(gate_part) * up_part).astype(jnp.bfloat16)
    expert_out = jnp.einsum(
        "erf,efd->erd",
        lax.all_gather(hidden, "tp", axis=2, tiled=True),
        down_serve,
        preferred_element_type=jnp.float32,
    ).astype(jnp.bfloat16)
    returned_rows = lax.all_to_all(expert_out, "fs", split_axis=1, concat_axis=0, tiled=True)
    picked = returned_rows.reshape(-1, returned_rows.shape[2])[targets].astype(jnp.float32)
    weighted = picked * route_weights.reshape(-1, 1)
    combined = jnp.sum(weighted.reshape(-1, 2, returned_rows.shape[2]), axis=1).astype(jnp.bfloat16)
    return (gate_serve, up_serve, down_serve, combined)


def solution(mesh):
    in_specs = (
        P(("grp", "fs"), None),
        P(("grp", "fs"), None),
        P(("grp", "fs"), None),
        P("fs"),
        P(None, "fs", "tp"),
        P(None, "fs", "tp"),
        P(None, "fs", "tp"),
    )
    out_specs = (
        P(("grp", "fs"), None, "tp"),
        P(("grp", "fs"), None, "tp"),
        P(("grp", "fs"), None, "tp"),
        P(("grp", "fs"), "tp"),
    )
    return jax.shard_map(
        on_device, mesh=mesh, in_specs=in_specs, out_specs=out_specs, check_vma=False
    )
```

profile of v0, /device:TPU:0, one launch (start us, length us, event | category | flops | bytes accessed | tf_op | source)
XLA Modules:
  0.0 250.0 jit_solution(12472034540438758420)
XLA Ops:
  7.2 1.5 convert_element_type.43
  11.9 3.5 %scatter_custom_fusion = bf16[1024,512]{1,0:T(8,128)(2,1)} fusion(s32[512]{0:T(512)S(1)} %bitcast.49, bf16[512,512]{1,0:T(8,128)(2,1)S(1)} %reshape.101, bf16[]{:T(256)} %constant.11.clone.1), kind=kCustom, calls=%fused_computation.11 | custom fusion | bytes 1048578 | tf_op jit(solution)/shard_map/scatter | solution.py:19
  15.4 6.3 %all-to-all-start.3 = ((bf16[8,128,512]{2,1,0:T(8,128)(2,1)}), bf16[8,128,512]{2,1,0:T(8,128)(2,1)S(1)}, u32[]{:S(2)}, u32[]{:S(2)}) async-start(bf16[8,128,512]{2,1,0:T(8,128)(2,1)} %bitcast.13), calls=%async_computation.3 | async-start | bytes 2097152 | tf_op jit(solution)/shard_map/all_to_all | solution.py:42
  21.7 6.5 %multiply_convert_fusion = (bf16[8,512,256]{2,1,0:T(8,128)(2,1)}, bf16[8,512,256]{2,1,0:T(8,128)(2,1)}) fusion(f32[8,512,256]{2,1,0:T(8,128)} %param.12, f32[512]{0:T(512)S(1)} %copy-done.4, f32[8,512,256]{2,1,0:T(8,128)} %param.11), kind=kLoop, calls=%fused_computation.2 | loop fusion | flops 4194304 | bytes 12584960 | tf_op jit(solution)/shard_map/convert_element_type | solution.py:26
  28.2 19.3 %all-to-all-done.3 = bf16[8,128,512]{2,1,0:T(8,128)(2,1)S(1)} async-done(((bf16[8,128,512]{2,1,0:T(8,128)(2,1)}), bf16[8,128,512]{2,1,0:T(8,128)(2,1)S(1)}, u32[]{:S(2)}, u32[]{:S(2)}) %all-to-all-start.3) | async-done | bytes 1048608 | tf_op jit(solution)/shard_map/all_to_all | solution.py:42
  47.5 3.6 %all-to-all-start = ((bf16[8,512,256]{2,1,0:T(8,128)(2,1)}), bf16[8,512,256]{2,1,0:T(8,128)(2,1)S(1)}, u32[]{:S(2)}, u32[]{:S(2)}) async-start(bf16[8,512,256]{2,1,0:T(8,128)(2,1)} %get-tuple-element.5), calls=%async_computation | async-start | bytes 4194304 | tf_op jit(solution)/shard_map/all_to_all | solution.py:29
  51.1 1.2 copy.31
  52.3 46.5 %all-to-all-done = bf16[8,512,256]{2,1,0:T(8,128)(2,1)S(1)} async-done(((bf16[8,512,256]{2,1,0:T(8,128)(2,1)}), bf16[8,512,256]{2,1,0:T(8,128)(2,1)S(1)}, u32[]{:S(2)}, u32[]{:S(2)}) %all-to-all-start) | async-done | bytes 2097184 | tf_op jit(solution)/shard_map/all_to_all | solution.py:29
  98.8 4.5 %all-to-all-start.1 = ((bf16[8,512,256]{2,1,0:T(8,128)(2,1)}), bf16[8,512,256]{2,1,0:T(8,128)(2,1)}, u32[]{:S(2)}, u32[]{:S(2)}) async-start(bf16[8,512,256]{2,1,0:T(8,128)(2,1)} %get-tuple-element.4), calls=%async_computation.1 | async-start | bytes 4194304 | tf_op jit(solution)/shard_map/all_to_all | solution.py:30
  103.3 3.8 %convert_element_type.40 = bf16[8,256,512]{2,1,0:T(8,128)(2,1)} convert(f32[8,256,512]{2,1,0:T(8,128)} %param.13) | non-fusion elementwise | flops 1048576 | bytes 6291456 | tf_op jit(solution)/shard_map/convert_element_type | solution.py:27
  107.0 1.5 copy.25
  108.5 42.6 %all-to-all-done.1 = bf16[8,512,256]{2,1,0:T(8,128)(2,1)} async-done(((bf16[8,512,256]{2,1,0:T(8,128)(2,1)}), bf16[8,512,256]{2,1,0:T(8,128)(2,1)}, u32[]{:S(2)}, u32[]{:S(2)}) %all-to-all-start.1) | async-done | bytes 2097184 | tf_op jit(solution)/shard_map/all_to_all | solution.py:30
  151.1 3.6 %all-to-all-start.2 = ((bf16[8,256,512]{2,1,0:T(8,128)(2,1)}), bf16[8,256,512]{2,1,0:T(8,128)(2,1)S(1)}, u32[]{:S(2)}, u32[]{:S(2)}) async-start(bf16[8,256,512]{2,1,0:T(8,128)(2,1)} %convert_element_type.40), calls=%async_computation.2 | async-start | bytes 4194304 | tf_op jit(solution)/shard_map/all_to_all | solution.py:31
  154.7 3.0 %copy.26 = bf16[4,2,512,256]{3,2,0,1:T(8,128)(2,1)} copy(bf16[4,2,512,256]{3,2,1,0:T(8,128)(2,1)} %bitcast.3) | data formatting | bytes 4194304 | tf_op jit(solution)/shard_map/all_to_all | solution.py:30
  157.8 4.2 %fusion.7 = f32[2,512,256]{2,1,0:T(8,128)S(1)} fusion(bf16[2,512,2048]{2,1,0:T(8,128)(2,1)} %all-gather.3.cloned.1.call-done, bf16[2,2048,256]{2,1,0:T(8,128)(2,1)} %bitcast.43), kind=kOutput, calls=%fused_computation.24 | convolution fusion | flops 1073741824 | bytes 7340032 | tf_op jit(solution)/shard_map/erd,edf->erf/dot_general | solution.py:50
  162.5 2.1 fusion
  164.6 37.8 %all-to-all-done.2 = bf16[8,256,512]{2,1,0:T(8,128)(2,1)S(1)} async-done(((bf16[8,256,512]{2,1,0:T(8,128)(2,1)}), bf16[8,256,512]{2,1,0:T(8,128)(2,1)S(1)}, u32[]{:S(2)}, u32[]{:S(2)}) %all-to-all-start.2) | async-done | bytes 2097184 | tf_op jit(solution)/shard_map/all_to_all | solution.py:31
  202.4 1.5 copy.27
  204.0 3.5 %convolution_convert_fusion = bf16[2,512,512]{2,1,0:T(8,128)(2,1)S(1)} fusion(bf16[2,512,1024]{2,1,0:T(8,128)(2,1)} %all-gather.5.cloned.1.call-done, bf16[2,1024,512]{2,1,0:T(8,128)(2,1)} %bitcast.47), kind=kOutput, calls=%fused_computation.5 | convolution fusion | flops 1074266112 | bytes 5242880 | tf_op jit(solution)/shard_map/erf,efd->erd/dot_general | solution.py:53
  207.4 2.0 copy.32
  209.5 3.7 %all-to-all-start.4 = ((bf16[2,512,512]{2,0,1:T(2,128)(2,1)}), bf16[2,512,512]{2,0,1:T(2,128)(2,1)S(1)}, u32[]{:S(2)}, u32[]{:S(2)}) async-start(bf16[2,512,512]{2,0,1:T(2,128)(2,1)} %copy.32), calls=%async_computation.4 | async-start | bytes 2097152 | tf_op jit(solution)/shard_map/all_to_all | solution.py:59
  213.4 24.9 %all-to-all-done.4 = bf16[2,512,512]{2,0,1:T(2,128)(2,1)S(1)} async-done(((bf16[2,512,512]{2,0,1:T(2,128)(2,1)}), bf16[2,512,512]{2,0,1:T(2,128)(2,1)S(1)}, u32[]{:S(2)}, u32[]{:S(2)}) %all-to-all-start.4) | async-done | bytes 1048608 | tf_op jit(solution)/shard_map/all_to_all | solution.py:59
  238.4 2.0 gather_fusion
  241.1 2.1 multiply_reduce_fusion.1
  (40 shorter events, 4.6 us)
Async XLA Ops:
  7.2 1.6 copy-start
  7.2 1.9 copy-start.2
  9.9 11.8 %copy-start.4 = (f32[512]{0:T(512)S(1)}, f32[512]{0:T(512)}, u32[]{:S(2)}) copy-start(f32[512]{0:T(512)} %param.10) | copy-start | bytes 6148
  15.4 32.1 %all-to-all-start.3 = ((bf16[8,128,512]{2,1,0:T(8,128)(2,1)}), bf16[8,128,512]{2,1,0:T(8,128)(2,1)S(1)}, u32[]{:S(2)}, u32[]{:S(2)}) async-start(bf16[8,128,512]{2,1,0:T(8,128)(2,1)} %bitcast.13), calls=%async_computation.3 | async-start | bytes 2097152 | tf_op jit(solution)/shard_map/all_to_all | solution.py:42
  47.5 51.3 %all-to-all-start = ((bf16[8,512,256]{2,1,0:T(8,128)(2,1)}), bf16[8,512,256]{2,1,0:T(8,128)(2,1)S(1)}, u32[]{:S(2)}, u32[]{:S(2)}) async-start(bf16[8,512,256]{2,1,0:T(8,128)(2,1)} %get-tuple-element.5), calls=%async_computation | async-start | bytes 4194304 | tf_op jit(solution)/shard_map/all_to_all | solution.py:29
  51.1 106.7 %all-gather.3.cloned.1.call-start = ((), (), s32[]{:S(2)}) async-start(), calls=%async_computation.5 | async-start | bytes 5242880 | tf_op jit(solution)/shard_map/all_gather | solution.py:49
  98.8 52.3 %all-to-all-start.1 = ((bf16[8,512,256]{2,1,0:T(8,128)(2,1)}), bf16[8,512,256]{2,1,0:T(8,128)(2,1)}, u32[]{:S(2)}, u32[]{:S(2)}) async-start(bf16[8,512,256]{2,1,0:T(8,128)(2,1)} %get-tuple-element.4), calls=%async_computation.1 | async-start | bytes 4194304 | tf_op jit(solution)/shard_map/all_to_all | solution.py:30
  151.1 51.3 %all-to-all-start.2 = ((bf16[8,256,512]{2,1,0:T(8,128)(2,1)}), bf16[8,256,512]{2,1,0:T(8,128)(2,1)S(1)}, u32[]{:S(2)}, u32[]{:S(2)}) async-start(bf16[8,256,512]{2,1,0:T(8,128)(2,1)} %convert_element_type.40), calls=%async_computation.2 | async-start | bytes 4194304 | tf_op jit(solution)/shard_map/all_to_all | solution.py:31
  154.7 49.3 %all-gather.5.cloned.1.call-start = ((), (), s32[]{:S(2)}) async-start(), calls=%async_computation.6 | async-start | bytes 2621440 | tf_op jit(solution)/shard_map/all_gather | solution.py:55
  157.8 4.3 %copy-start.1 = (bf16[4,2,512,256]{3,2,0,1:T(8,128)(2,1)S(1)}, bf16[4,2,512,256]{3,2,0,1:T(8,128)(2,1)}, u32[]{:S(2)}) copy-start(bf16[4,2,512,256]{3,2,0,1:T(8,128)(2,1)} %copy.26) | copy-start | bytes 6291460
  157.8 4.7 %copy-start.5 = (bf16[2,512,2048]{2,1,0:T(8,128)(2,1)S(1)}, bf16[2,512,2048]{2,1,0:T(8,128)(2,1)}, u32[]{:S(2)}) copy-start(bf16[2,512,2048]{2,1,0:T(8,128)(2,1)} %all-gather.3.cloned.1.call-done) | copy-start | bytes 12582916
  207.4 5.8 %copy-start.3 = (f32[256,2]{0,1:T(2,128)S(1)}, f32[256,2]{0,1:T(2,128)}, u32[]{:S(2)}) copy-start(f32[256,2]{0,1:T(2,128)} %param.9) | copy-start | bytes 6148
  209.5 28.8 %all-to-all-start.4 = ((bf16[2,512,512]{2,0,1:T(2,128)(2,1)}), bf16[2,512,512]{2,0,1:T(2,128)(2,1)S(1)}, u32[]{:S(2)}, u32[]{:S(2)}) async-start(bf16[2,512,512]{2,0,1:T(2,128)(2,1)} %copy.32), calls=%async_computation.4 | async-start | bytes 2097152 | tf_op jit(solution)/shard_map/all_to_all | solution.py:59
Sparse Core Ops, SparseCore 0:
  53.5 35.8 all-gather.2
  164.8 24.1 all-gather.4
where the time goes:
time: 251 us; the launch traced here: 250 us
  waiting for transfers between devices  171 us (68%)
  starting transfers between devices  21.8 us (9%)
  local copies, waits for them, and re-layouts  17.5 us (7%)
  other arithmetic  15.5 us (6%)
  between operations  14.3 us (6%)
  matrix products  9.85 us (4%)
    all_to_all x1, waiting for transfers between devices, on_device(): lax.all_to_all(gate_local, 'fs', split_axis=0, concat_axis=1, tiled=True)  46.5 us
    all_to_all x1, waiting for transfers between devices, on_device(): lax.all_to_all(up_local, 'fs', split_axis=0, concat_axis=1, tiled=True)  42.6 us
    all_to_all x1, waiting for transfers between devices, on_device(): lax.all_to_all(down_local, 'fs', split_axis=0, concat_axis=1, tiled=True)  37.8 us
    all_to_all x1, waiting for transfers between devices, on_device(): lax.all_to_all(expert_out, 'fs', split_axis=1, concat_axis=0, tiled=True)  24.9 us
    all_to_all x1, waiting for transfers between devices, on_device(): lax.all_to_all(fill_slots(own_cols, targets, experts, capacity), 'fs', sp...  19.3 us
    convert_element_type x1, other arithmetic, on_device(): up_local = (up_master * row_gain).astype(jnp.bfloat16)  6.46 us
    all_to_all x1, starting transfers between devices, on_device(): lax.all_to_all(fill_slots(own_cols, targets, experts, capacity), 'fs', sp...  6.35 us
  transfers between devices with their start and end apart: 7, of which 5 were waited for; matrix products, arithmetic and copies ran while one was open for 10% of the time, Pallas kernels for 0%

commit v1 on v0

--- a/solution.py
+++ b/solution.py
@@ -39,13 +39,20 @@
     targets = slot_targets(route_ids, experts, capacity)
     col_width = normed.shape[1] // lax.axis_size("tp")
     own_cols = lax.dynamic_slice_in_dim(normed, lax.axis_index("tp") * col_width, col_width, 1)
-    part_rows = lax.all_to_all(
-        fill_slots(own_cols, targets, experts, capacity),
-        "fs",
-        split_axis=0,
-        concat_axis=1,
-        tiled=True,
-    )
+    array = fill_slots(own_cols, targets, experts, capacity)
+    ways, here = (lax.axis_size("fs"), lax.axis_index("fs"))
+    width = array.shape[0] // ways
+    dims = list(array.shape)
+    dims[0] = width
+    height = dims[1]
+    dims[1] = height * ways
+    full = jnp.zeros(dims, array.dtype)
+    for mask in range(ways):
+        part = lax.dynamic_slice_in_dim(array, (here ^ mask) * width, width, axis=0)
+        if mask:
+            part = lax.ppermute(part, "fs", [(d, d ^ mask) for d in range(ways)])
+        full = lax.dynamic_update_slice_in_dim(full, part, (here ^ mask) * height, axis=1)
+    part_rows = full
     portion = lax.all_gather(part_rows, "tp", axis=2, tiled=True)
     gate_part = jnp.einsum("erd,edf->erf", portion, gate_serve, preferred_element_type=jnp.float32)
     up_part = jnp.einsum("erd,edf->erf", portion, up_serve, preferred_element_type=jnp.float32)

time: 251 us -> 241 us (0.960)
  waiting for transfers between devices: 171 us -> 158 us
    all_to_all x1 -> x0, waiting for transfers between devices: 19.3 us -> none  [on_device(): lax.all_to_all(fill_slots(own_cols, targets, experts, capacity), 'fs', sp...]
    ppermute x0 -> x3, waiting for transfers between devices: none -> 17.8 us  [on_device(): part = lax.ppermute(part, 'fs', [(d, d ^ mask) for d in range(ways)])]
    all_to_all x1, waiting for transfers between devices: 46.5 us -> 35.8 us  [on_device(): lax.all_to_all(gate_local, 'fs', split_axis=0, concat_axis=1, tiled=True)]
    all_to_all x1 -> x0, starting transfers between devices: 6.35 us -> none  [on_device(): lax.all_to_all(fill_slots(own_cols, targets, experts, capacity), 'fs', sp...]
    ppermute x0 -> x3, starting transfers between devices: none -> 5.64 us  [on_device(): part = lax.ppermute(part, 'fs', [(d, d ^ mask) for d in range(ways)])]
  transfers between devices with their start and end apart: 7 -> 9, of which waited for: 5 -> 5; matrix products, arithmetic and copies ran while one was open for 10% -> 10% of each run, Pallas kernels for 0% -> 0%
where the time goes in v1:
time: 241 us; the launch traced here: 240 us
  waiting for transfers between devices  158 us (66%)
  starting transfers between devices  22.6 us (9%)
  local copies, waits for them, and re-layouts  19.6 us (8%)
  other arithmetic  15.5 us (6%)
  between operations  14.3 us (6%)
  matrix products  9.86 us (4%)
    all_to_all x1, waiting for transfers between devices, on_device(): lax.all_to_all(up_local, 'fs', split_axis=0, concat_axis=1, tiled=True)  42.2 us
    all_to_all x1, waiting for transfers between devices, on_device(): lax.all_to_all(down_local, 'fs', split_axis=0, concat_axis=1, tiled=True)  37.8 us
    all_to_all x1, waiting for transfers between devices, on_device(): lax.all_to_all(gate_local, 'fs', split_axis=0, concat_axis=1, tiled=True)  35.8 us
    all_to_all x1, waiting for transfers between devices, on_device(): lax.all_to_all(expert_out, 'fs', split_axis=1, concat_axis=0, tiled=True)  24.9 us
    ppermute x3, waiting for transfers between devices, on_device(): part = lax.ppermute(part, 'fs', [(d, d ^ mask) for d in range(ways)])  17.8 us
    convert_element_type x1, other arithmetic, on_device(): up_local = (up_master * row_gain).astype(jnp.bfloat16)  6.46 us
    ppermute x3, starting transfers between devices, on_device(): part = lax.ppermute(part, 'fs', [(d, d ^ mask) for d in range(ways)])  5.64 us
    all_to_all x1, starting transfers between devices, on_device(): lax.all_to_all(gate_local, 'fs', split_axis=0, concat_axis=1, tiled=True)  5.09 us
  transfers between devices with their start and end apart: 9, of which 5 were waited for; matrix products, arithmetic and copies ran while one was open for 10% of the time, Pallas kernels for 0%

profile of v1, /device:TPU:0, one launch (start us, length us, event | category | flops | bytes accessed | tf_op | source)
XLA Modules:
  0.0 240.3 jit_solution(7443260357843464789)
XLA Ops:
  7.2 1.5 convert_element_type.43
  11.9 2.7 %scatter_custom_fusion = bf16[1024,512]{1,0:T(8,128)(2,1)S(1)} fusion(s32[512]{0:T(512)S(1)} %bitcast.44, bf16[512,512]{1,0:T(8,128)(2,1)S(1)} %reshape.101, bf16[]{:T(256)} %constant.16.clone.1), kind=kCustom, calls=%fused_computation.10 | custom fusion | bytes 1048578 | tf_op jit(solution)/shard_map/scatter | solution.py:19
  15.7 3.1 %collective-permute-start = (bf16[2,128,512]{2,1,0:T(8,128)(2,1)}, bf16[2,128,512]{2,1,0:T(8,128)(2,1)}, u32[]{:S(2)}, u32[]{:S(2)}) collective-permute-start(bf16[2,128,512]{2,1,0:T(8,128)(2,1)} %get-tuple-element.6), channel_id=1, source_target_pairs={{0,4},{4,0},{8,12},{12,8},{1,5},{5,1},{9,13},{13,9},{2,6},{6,2},{1... | collective-permute-start | bytes 786440 | tf_op jit(solution)/shard_map/ppermute | solution.py:53
  18.7 2.6 %collective-permute-start.1 = (bf16[2,128,512]{2,1,0:T(8,128)(2,1)}, bf16[2,128,512]{2,1,0:T(8,128)(2,1)}, u32[]{:S(2)}, u32[]{:S(2)}) collective-permute-start(bf16[2,128,512]{2,1,0:T(8,128)(2,1)} %get-tuple-element.5), channel_id=1, source_target_pairs={{0,8},{4,12},{8,0},{12,4},{1,9},{5,13},{9,1},{13,5},{2,10},{6,14},... | collective-permute-start | bytes 786440 | tf_op jit(solution)/shard_map/ppermute | solution.py:53
  21.3 6.5 %multiply_convert_fusion = (bf16[8,512,256]{2,1,0:T(8,128)(2,1)}, bf16[8,512,256]{2,1,0:T(8,128)(2,1)}) fusion(f32[8,512,256]{2,1,0:T(8,128)} %param.12, f32[512]{0:T(512)S(1)} %copy-done.5, f32[8,512,256]{2,1,0:T(8,128)} %param.11), kind=kLoop, calls=%fused_computation.2 | loop fusion | flops 4194304 | bytes 12584960 | tf_op jit(solution)/shard_map/convert_element_type | solution.py:26
  27.8 5.1 %all-to-all-start = ((bf16[8,512,256]{2,1,0:T(8,128)(2,1)}), bf16[8,512,256]{2,1,0:T(8,128)(2,1)S(1)}, u32[]{:S(2)}, u32[]{:S(2)}) async-start(bf16[8,512,256]{2,1,0:T(8,128)(2,1)} %get-tuple-element.9), calls=%async_computation | async-start | bytes 4194304 | tf_op jit(solution)/shard_map/all_to_all | solution.py:29
  33.9 17.8 %collective-permute-done.1 = bf16[2,128,512]{2,1,0:T(8,128)(2,1)} collective-permute-done((bf16[2,128,512]{2,1,0:T(8,128)(2,1)}, bf16[2,128,512]{2,1,0:T(8,128)(2,1)}, u32[]{:S(2)}, u32[]{:S(2)}) %collective-permute-start.1) | collective-permute-done | bytes 262176 | tf_op jit(solution)/shard_map/ppermute | solution.py:53
  53.7 35.8 %all-to-all-done = bf16[8,512,256]{2,1,0:T(8,128)(2,1)S(1)} async-done(((bf16[8,512,256]{2,1,0:T(8,128)(2,1)}), bf16[8,512,256]{2,1,0:T(8,128)(2,1)S(1)}, u32[]{:S(2)}, u32[]{:S(2)}) %all-to-all-start) | async-done | bytes 2097184 | tf_op jit(solution)/shard_map/all_to_all | solution.py:29
  89.5 4.5 %all-to-all-start.1 = ((bf16[8,512,256]{2,1,0:T(8,128)(2,1)}), bf16[8,512,256]{2,1,0:T(8,128)(2,1)}, u32[]{:S(2)}, u32[]{:S(2)}) async-start(bf16[8,512,256]{2,1,0:T(8,128)(2,1)} %get-tuple-element.8), calls=%async_computation.1 | async-start | bytes 4194304 | tf_op jit(solution)/shard_map/all_to_all | solution.py:30
  94.0 3.8 %convert_element_type.40 = bf16[8,256,512]{2,1,0:T(8,128)(2,1)} convert(f32[8,256,512]{2,1,0:T(8,128)} %param.13) | non-fusion elementwise | flops 1048576 | bytes 6291456 | tf_op jit(solution)/shard_map/convert_element_type | solution.py:27
  97.7 1.5 copy.24
  99.2 42.2 %all-to-all-done.1 = bf16[8,512,256]{2,1,0:T(8,128)(2,1)} async-done(((bf16[8,512,256]{2,1,0:T(8,128)(2,1)}), bf16[8,512,256]{2,1,0:T(8,128)(2,1)}, u32[]{:S(2)}, u32[]{:S(2)}) %all-to-all-start.1) | async-done | bytes 2097184 | tf_op jit(solution)/shard_map/all_to_all | solution.py:30
  141.4 3.6 %all-to-all-start.2 = ((bf16[8,256,512]{2,1,0:T(8,128)(2,1)}), bf16[8,256,512]{2,1,0:T(8,128)(2,1)S(1)}, u32[]{:S(2)}, u32[]{:S(2)}) async-start(bf16[8,256,512]{2,1,0:T(8,128)(2,1)} %convert_element_type.40), calls=%async_computation.2 | async-start | bytes 4194304 | tf_op jit(solution)/shard_map/all_to_all | solution.py:31
  145.1 3.0 %copy.25 = bf16[4,2,512,256]{3,2,0,1:T(8,128)(2,1)} copy(bf16[4,2,512,256]{3,2,1,0:T(8,128)(2,1)} %bitcast.3) | data formatting | bytes 4194304 | tf_op jit(solution)/shard_map/all_to_all | solution.py:30
  148.1 4.2 %fusion.6 = f32[2,512,256]{2,1,0:T(8,128)S(1)} fusion(bf16[2,512,2048]{2,1,0:T(8,128)(2,1)} %all-gather.3.cloned.1.call-done, bf16[2,2048,256]{2,1,0:T(8,128)(2,1)} %bitcast.38), kind=kOutput, calls=%fused_computation.30 | convolution fusion | flops 1073741824 | bytes 7340032 | tf_op jit(solution)/shard_map/erd,edf->erf/dot_general | solution.py:57
  152.8 2.1 multiply_convert_fusion.2
  155.0 37.8 %all-to-all-done.2 = bf16[8,256,512]{2,1,0:T(8,128)(2,1)S(1)} async-done(((bf16[8,256,512]{2,1,0:T(8,128)(2,1)}), bf16[8,256,512]{2,1,0:T(8,128)(2,1)S(1)}, u32[]{:S(2)}, u32[]{:S(2)}) %all-to-all-start.2) | async-done | bytes 2097184 | tf_op jit(solution)/shard_map/all_to_all | solution.py:31
  192.7 1.5 copy.26
  194.3 3.5 %convolution_convert_fusion = bf16[2,512,512]{2,1,0:T(8,128)(2,1)S(1)} fusion(bf16[2,512,1024]{2,1,0:T(8,128)(2,1)} %all-gather.5.cloned.1.call-done, bf16[2,1024,512]{2,1,0:T(8,128)(2,1)} %bitcast.42), kind=kOutput, calls=%fused_computation.5 | convolution fusion | flops 1074266112 | bytes 5242880 | tf_op jit(solution)/shard_map/erf,efd->erd/dot_general | solution.py:60
  197.8 2.1 copy.30
  199.8 3.7 %all-to-all-start.3 = ((bf16[2,512,512]{2,0,1:T(2,128)(2,1)}), bf16[2,512,512]{2,0,1:T(2,128)(2,1)S(1)}, u32[]{:S(2)}, u32[]{:S(2)}) async-start(bf16[2,512,512]{2,0,1:T(2,128)(2,1)} %copy.30), calls=%async_computation.3 | async-start | bytes 2097152 | tf_op jit(solution)/shard_map/all_to_all | solution.py:66
  203.7 24.9 %all-to-all-done.3 = bf16[2,512,512]{2,0,1:T(2,128)(2,1)S(1)} async-done(((bf16[2,512,512]{2,0,1:T(2,128)(2,1)}), bf16[2,512,512]{2,0,1:T(2,128)(2,1)S(1)}, u32[]{:S(2)}, u32[]{:S(2)}) %all-to-all-start.3) | async-done | bytes 1048608 | tf_op jit(solution)/shard_map/all_to_all | solution.py:66
  228.8 2.0 gather_fusion
  231.4 2.1 multiply_reduce_fusion.1
  (50 shorter events, 8.6 us)
Async XLA Ops:
  7.2 1.6 copy-start
  7.2 1.9 copy-start.3
  11.9 9.4 %copy-start.5 = (f32[512]{0:T(512)S(1)}, f32[512]{0:T(512)}, u32[]{:S(2)}) copy-start(f32[512]{0:T(512)} %param.10) | copy-start | bytes 6148
  15.7 17.2 %collective-permute-start = (bf16[2,128,512]{2,1,0:T(8,128)(2,1)}, bf16[2,128,512]{2,1,0:T(8,128)(2,1)}, u32[]{:S(2)}, u32[]{:S(2)}) collective-permute-start(bf16[2,128,512]{2,1,0:T(8,128)(2,1)} %get-tuple-element.6), channel_id=1, source_target_pairs={{0,4},{4,0},{8,12},{12,8},{1,5},{5,1},{9,13},{13,9},{2,6},{6,2},{1... | collective-permute-start | bytes 786440 | tf_op jit(solution)/shard_map/ppermute | solution.py:53
  18.7 32.9 %collective-permute-start.1 = (bf16[2,128,512]{2,1,0:T(8,128)(2,1)}, bf16[2,128,512]{2,1,0:T(8,128)(2,1)}, u32[]{:S(2)}, u32[]{:S(2)}) collective-permute-start(bf16[2,128,512]{2,1,0:T(8,128)(2,1)} %get-tuple-element.5), channel_id=1, source_target_pairs={{0,8},{4,12},{8,0},{12,4},{1,9},{5,13},{9,1},{13,5},{2,10},{6,14},... | collective-permute-start | bytes 786440 | tf_op jit(solution)/shard_map/ppermute | solution.py:53
  21.3 31.3 %collective-permute-start.2 = (bf16[2,128,512]{2,1,0:T(8,128)(2,1)}, bf16[2,128,512]{2,1,0:T(8,128)(2,1)S(1)}, u32[]{:S(2)}, u32[]{:S(2)}) collective-permute-start(bf16[2,128,512]{2,1,0:T(8,128)(2,1)} %get-tuple-element.4), channel_id=1, source_target_pairs={{0,12},{4,8},{8,4},{12,0},{1,13},{5,9},{9,5},{13,1},{2,14},{6,10},... | collective-permute-start | bytes 786440 | tf_op jit(solution)/shard_map/ppermute | solution.py:53
  27.8 61.7 %all-to-all-start = ((bf16[8,512,256]{2,1,0:T(8,128)(2,1)}), bf16[8,512,256]{2,1,0:T(8,128)(2,1)S(1)}, u32[]{:S(2)}, u32[]{:S(2)}) async-start(bf16[8,512,256]{2,1,0:T(8,128)(2,1)} %get-tuple-element.9), calls=%async_computation | async-start | bytes 4194304 | tf_op jit(solution)/shard_map/all_to_all | solution.py:29
  32.9 115.2 %all-gather.3.cloned.1.call-start = ((), (), s32[]{:S(2)}) async-start(), calls=%async_computation.4 | async-start | bytes 5242880 | tf_op jit(solution)/shard_map/all_gather | solution.py:56
  52.6 1.1 copy-start.1
  89.5 51.9 %all-to-all-start.1 = ((bf16[8,512,256]{2,1,0:T(8,128)(2,1)}), bf16[8,512,256]{2,1,0:T(8,128)(2,1)}, u32[]{:S(2)}, u32[]{:S(2)}) async-start(bf16[8,512,256]{2,1,0:T(8,128)(2,1)} %get-tuple-element.8), calls=%async_computation.1 | async-start | bytes 4194304 | tf_op jit(solution)/shard_map/all_to_all | solution.py:30
  141.4 51.3 %all-to-all-start.2 = ((bf16[8,256,512]{2,1,0:T(8,128)(2,1)}), bf16[8,256,512]{2,1,0:T(8,128)(2,1)S(1)}, u32[]{:S(2)}, u32[]{:S(2)}) async-start(bf16[8,256,512]{2,1,0:T(8,128)(2,1)} %convert_element_type.40), calls=%async_computation.2 | async-start | bytes 4194304 | tf_op jit(solution)/shard_map/all_to_all | solution.py:31
  145.0 49.3 %all-gather.5.cloned.1.call-start = ((), (), s32[]{:S(2)}) async-start(), calls=%async_computation.5 | async-start | bytes 2621440 | tf_op jit(solution)/shard_map/all_gather | solution.py:62
  148.1 4.3 %copy-start.2 = (bf16[4,2,512,256]{3,2,0,1:T(8,128)(2,1)S(1)}, bf16[4,2,512,256]{3,2,0,1:T(8,128)(2,1)}, u32[]{:S(2)}) copy-start(bf16[4,2,512,256]{3,2,0,1:T(8,128)(2,1)} %copy.25) | copy-start | bytes 6291460
  148.1 4.7 %copy-start.6 = (bf16[2,512,2048]{2,1,0:T(8,128)(2,1)S(1)}, bf16[2,512,2048]{2,1,0:T(8,128)(2,1)}, u32[]{:S(2)}) copy-start(bf16[2,512,2048]{2,1,0:T(8,128)(2,1)} %all-gather.3.cloned.1.call-done) | copy-start | bytes 12582916
  197.8 5.8 %copy-start.4 = (f32[256,2]{0,1:T(2,128)S(1)}, f32[256,2]{0,1:T(2,128)}, u32[]{:S(2)}) copy-start(f32[256,2]{0,1:T(2,128)} %param.9) | copy-start | bytes 6148
  199.8 28.8 %all-to-all-start.3 = ((bf16[2,512,512]{2,0,1:T(2,128)(2,1)}), bf16[2,512,512]{2,0,1:T(2,128)(2,1)S(1)}, u32[]{:S(2)}, u32[]{:S(2)}) async-start(bf16[2,512,512]{2,0,1:T(2,128)(2,1)} %copy.30), calls=%async_computation.3 | async-start | bytes 2097152 | tf_op jit(solution)/shard_map/all_to_all | solution.py:66
Sparse Core Ops, SparseCore 0:
  53.8 37.1 all-gather.2
  155.1 24.1 all-gather.4
